TPU v7x, 32 devices: a whole 2x2x4 slice. The times are simulated.
32 devices in a mesh: sp: 8 (over z, x), tp: 4 (over y, core).
Axes of the slice: x: 2, y: 2, z: 4, core: 2. Of those that a mesh axis runs over, the one named last changes fastest.
Arguments:
- tokens: bfloat16 [2048, 1024], P(('sp', 'tp')), may hold values from -6 to 6
- doc_ids: int32 [2048], P('sp'), may hold values from 0 to 7, never falling along the last dimension, each value on 1 to 1536 neighbouring positions
- down_query: bfloat16 [1024, 256], P('sp'), may hold values from -0.1875 to 0.1875
- down_key: bfloat16 [1024, 256], P('sp'), may hold values from -0.1875 to 0.1875
- down_rotary: bfloat16 [1024, 32], P('sp'), may hold values from -0.1875 to 0.1875
- query_gain: float32 [256], replicated, may hold values from 0.1 to 1.9
- key_gain: float32 [256], replicated, may hold values from 0.1 to 1.9
- up_query: bfloat16 [256, 1536], P('sp', 'tp'), may hold values from -0.375 to 0.375
- up_key: bfloat16 [256, 1024], P('sp', 'tp'), may hold values from -0.375 to 0.375
- up_value: bfloat16 [256, 1024], P('sp', 'tp'), may hold values from -0.375 to 0.375
- output_weight: bfloat16 [1024, 1024], P('tp', 'sp'), may hold values from -0.1875 to 0.1875
- out_gain: float32 [1024], replicated, may hold values from 0.1 to 1.9
Outputs:
- mixed: bfloat16 [2048, 1024], P(('sp', 'tp'))
- log_sums: float32 [2048, 16], P('sp', 'tp')
Inputs may be any that keep to these rules, and one draw needn't show every extreme that they name: doc_ids never fall along the sequence and run from 0 to at most the number of devices along sp minus one; each document has 1 to 1536 positions, and one document has exactly that many.
All inputs are finite; a program needn't handle non-finite values.
Results may differ from a plain program's by a relative error of at most 0.02.
Values may be sent and summed in bfloat16 or wider, within the bound.
A program may use at most 64 MiB of HBM per device.

v0:
```python
import math

import jax
import jax.numpy as jnp
from jax import lax
from jax.sharding import PartitionSpec as P

NOPE = 64
ROPE = 32
VDIM = 64


NEG_BIG = -1e30
THETA = 10000.0
EPS = 1e-06


def folded(value, axis, dim, absorb, carry):
    whole = jax.tree.map(lambda part: lax.all_gather(part, axis, axis=dim, tiled=True), value)
    return absorb(carry, whole, jnp.int32(0))


def gathered_then(value, axis, dim, block):
    whole = lax.all_gather(value, axis, axis=dim, tiled=True)
    return block(whole, jnp.int32(0))


def summed_rows(product, extent, axis):
    everything = product(jnp.int32(0), lax.axis_size(axis) * extent)
    own = lax.psum_scatter(everything.astype(jnp.bfloat16), axis, scatter_dimension=0, tiled=True)
    return own.astype(jnp.float32)


def settle(quantity):
    return lax.optimization_barrier(quantity.astype(jnp.bfloat16))


def rms_gain(summed, gain_vector):
    widened = settle(summed).astype(jnp.float32)
    scaled = widened * lax.rsqrt(jnp.mean(widened * widened, axis=-1, keepdims=True) + EPS)
    return (scaled * gain_vector).astype(jnp.bfloat16)


def rotate(vectors, positions):
    half_width = vectors.shape[-1] // 2
    inverse = THETA ** (-jnp.arange(half_width, dtype=jnp.float32) / half_width)
    angles = positions.astype(jnp.float32)[:, None] * inverse[None, :]
    angles = angles.reshape((vectors.shape[0],) + (1,) * (vectors.ndim - 2) + (half_width,))
    cosine_part = jnp.cos(angles)
    sine_part = jnp.sin(angles)
    widened = vectors.astype(jnp.float32)
    front_half = widened[..., :half_width]
    back_half = widened[..., half_width:]
    return jnp.concatenate(
        [
            front_half * cosine_part - back_half * sine_part,
            back_half * cosine_part + front_half * sine_part,
        ],
        axis=-1,
    ).astype(jnp.bfloat16)


def over_blocks(carry, arrays, block_size, one_step):
    length = arrays[0].shape[0]
    if length == block_size:
        return one_step(carry, arrays)
    pieces_split = tuple(
        (array.reshape((length // block_size, block_size) + array.shape[1:]) for array in arrays)
    )

    def advance(carried, blocks):
        return (one_step(carried, blocks), None)

    carry, unused = lax.scan(advance, carry, pieces_split)
    return carry


def on_device(
    tokens,
    doc_ids,
    down_query,
    down_key,
    down_rotary,
    query_gain,
    key_gain,
    up_query,
    up_key,
    up_value,
    output_weight,
    out_gain,
):
    own_rows = tokens.shape[0]
    block_len = doc_ids.shape[0]
    local_heads = up_key.shape[1] // NOPE
    sp_base = lax.axis_index("sp") * block_len
    tp_first = lax.axis_index("tp") * own_rows
    row_pos = sp_base + tp_first + jnp.arange(own_rows, dtype=jnp.int32)
    score_scale = 1.0 / math.sqrt(NOPE + ROPE)

    def add_down(totals, pieces, offset):
        columns = lax.dynamic_slice_in_dim(tokens, offset, pieces[0].shape[0], 1)
        return tuple(
            (
                running + jnp.dot(columns, portion, preferred_element_type=jnp.float32)
                for running, portion in zip(totals, pieces)
            )
        )

    initial = tuple(
        (
            jnp.zeros((own_rows, weight.shape[1]), jnp.float32)
            for weight in (down_query, down_key, down_rotary)
        )
    )
    query_sum, latent_sum, rotary_sum = folded(
        (down_query, down_key, down_rotary), "sp", 0, add_down, initial
    )
    query_latent = rms_gain(query_sum, query_gain)
    key_latent = rms_gain(latent_sum, key_gain)
    key_rot = rotate(settle(rotary_sum), row_pos)
    query_up, key_up, value_up = (
        lax.all_gather(up_query, "sp", axis=0, tiled=True),
        lax.all_gather(up_key, "sp", axis=0, tiled=True),
        lax.all_gather(up_value, "sp", axis=0, tiled=True),
    )

    def make_queries(portion, offset):
        length = portion.shape[0]
        positions = sp_base + offset + jnp.arange(length, dtype=jnp.int32)
        projected = settle(jnp.dot(portion, query_up, preferred_element_type=jnp.float32))
        projected = projected.reshape(length, local_heads, NOPE + ROPE)
        turned = rotate(projected[..., NOPE:], positions)
        joined_query = jnp.concatenate([projected[..., :NOPE], turned], axis=-1)
        return joined_query.reshape(length, local_heads * (NOPE + ROPE))

    queries = gathered_then(query_latent, "tp", 0, make_queries)
    queries = queries.reshape(block_len, local_heads, NOPE + ROPE)
    query_plain = queries[..., :NOPE]
    query_turned = queries[..., NOPE:]
    query_docs = doc_ids.astype(jnp.float32)

    def attend(carry, key_plain, key_turned, values, key_docs):
        top_score, weight_sum, accumulated = carry
        scores = jnp.einsum(
            "qhd,khd->hqk", query_plain, key_plain, preferred_element_type=jnp.float32
        )
        scores = scores + jnp.einsum(
            "qhr,kr->hqk", query_turned, key_turned, preferred_element_type=jnp.float32
        )
        scores = scores * score_scale
        same_doc = (query_docs[:, None] == key_docs[None, :])[None]
        new_top = jnp.maximum(top_score, jnp.max(jnp.where(same_doc, scores, NEG_BIG), axis=-1))
        weights = jnp.where(same_doc, jnp.exp(scores - new_top[..., None]), 0.0)
        rescale = jnp.exp(top_score - new_top)
        weight_sum = weight_sum * rescale + jnp.sum(weights, axis=-1)
        accumulated = accumulated * rescale.T[:, :, None] + jnp.einsum(
            "hqk,khv->qhv", weights.astype(jnp.bfloat16), values, preferred_element_type=jnp.float32
        )
        return (new_top, weight_sum, accumulated)

    def guarded(carry, key_plain, key_turned, values, key_docs):
        return attend(carry, key_plain, key_turned, values, key_docs)

    start_state = (
        jnp.full((local_heads, block_len), NEG_BIG, jnp.float32),
        jnp.zeros((local_heads, block_len), jnp.float32),
        jnp.zeros((block_len, local_heads, VDIM), jnp.float32),
    )
    latent_width = key_latent.shape[1]
    joined = jnp.concatenate([key_latent, key_rot], axis=1)

    def expand_rows(portion, offset):
        latent_rows = portion[:, :latent_width]
        turned_rows = portion[:, latent_width:]
        key_plain = jnp.dot(latent_rows, key_up, preferred_element_type=jnp.float32).astype(
            jnp.bfloat16
        )
        values = jnp.dot(latent_rows, value_up, preferred_element_type=jnp.float32).astype(
            jnp.bfloat16
        )
        return jnp.concatenate([key_plain, values, turned_rows], axis=1)

    expanded = gathered_then(joined, "tp", 0, expand_rows)

    def fold_expanded(carry, pieces, offset):

        def one_step(carried, blocks):
            rows_block, docs_rows = blocks
            length = rows_block.shape[0]
            plain_end = local_heads * NOPE
            value_end = local_heads * (NOPE + VDIM)
            key_plain = rows_block[:, :plain_end].reshape(length, local_heads, NOPE)
            values = rows_block[:, plain_end:value_end].reshape(length, local_heads, VDIM)
            turned_rows = rows_block[:, value_end:]
            return guarded(carried, key_plain, turned_rows, values, docs_rows.astype(jnp.float32))

        return over_blocks(carry, pieces, math.gcd(pieces[0].shape[0], block_len), one_step)

    carry = folded((expanded, doc_ids.astype(jnp.bfloat16)), "sp", 0, fold_expanded, start_state)
    top_score, weight_sum, accumulated = carry
    log_sums = (top_score + jnp.log(weight_sum)).T
    attended = (accumulated / weight_sum.T[:, :, None]).astype(jnp.bfloat16)
    attended = attended.reshape(block_len, local_heads * VDIM)
    output_full = lax.all_gather(output_weight, "sp", axis=1, tiled=True)

    def project(offset, length):
        return jnp.dot(
            lax.dynamic_slice_in_dim(attended, offset, length, 0),
            output_full,
            preferred_element_type=jnp.float32,
        )

    summed = summed_rows(project, own_rows, "tp")
    return (rms_gain(summed, out_gain), log_sums)


def solution(mesh):
    placed = (
        P(("sp", "tp"), None),
        P("sp"),
        P("sp", None),
        P("sp", None),
        P("sp", None),
        P(),
        P(),
        P("sp", "tp"),
        P("sp", "tp"),
        P("sp", "tp"),
        P("tp", "sp"),
        P(),
    )
    return jax.shard_map(
        on_device,
        mesh=mesh,
        in_specs=placed,
        out_specs=(P(("sp", "tp"), None), P("sp", "tp")),
        check_vma=False,
    )
```

profile of v0, /device:TPU:0, one launch (start us, length us, event | category | flops | bytes accessed | tf_op | source)
XLA Modules:
  0.0 315.1 jit_solution(16009632150641457228)
XLA Ops:
  7.3 32.6 %all_gather.35 = bf16[1024,32]{0,1:T(8,128)(2,1)S(1)} all-gather(bf16[128,32]{0,1:T(8,128)(2,1)} %param.18), channel_id=1, replica_groups=mesh['sp'=8,'tp'=4] {'sp'}, dimensions={0}, use_global_device_ids=true | all-gather | bytes 73728 | tf_op jit(solution)/shard_map/all_gather | solution.py:19
  40.4 31.4 %all_gather.34 = bf16[1024,256]{1,0:T(8,128)(2,1)S(1)} all-gather(bf16[128,256]{1,0:T(8,128)(2,1)} %param.17), channel_id=1, replica_groups=mesh['sp'=8,'tp'=4] {'sp'}, dimensions={0}, use_global_device_ids=true | all-gather | bytes 589824 | tf_op jit(solution)/shard_map/all_gather | solution.py:19
  72.1 0.8 fusion.19
  73.0 5.6 %all_gather.36 = bf16[256,288]{1,0:T(8,128)(2,1)S(1)} all-gather(bf16[64,288]{1,0:T(8,128)(2,1)S(1)} %pad_maximum_fusion.2), channel_id=1, replica_groups=mesh['sp'=8,'tp'=4] {'tp'}, dimensions={0}, use_global_device_ids=true | all-gather | bytes 184320 | tf_op jit(solution)/shard_map/all_gather | solution.py:24
  78.6 30.7 %all_gather.38 = bf16[256,256]{1,0:T(8,128)(2,1)S(1)} all-gather(bf16[32,256]{1,0:T(8,128)(2,1)} %param.23), channel_id=1, replica_groups=mesh['sp'=8,'tp'=4] {'sp'}, dimensions={0}, use_global_device_ids=true | all-gather | bytes 147456 | tf_op jit(solution)/shard_map/all_gather | solution.py:124
  109.6 30.5 %all_gather.37 = bf16[256,256]{1,0:T(8,128)(2,1)S(1)} all-gather(bf16[32,256]{1,0:T(8,128)(2,1)S(1)} %copy-done.4), channel_id=1, replica_groups=mesh['sp'=8,'tp'=4] {'sp'}, dimensions={0}, use_global_device_ids=true | all-gather | bytes 147456 | tf_op jit(solution)/shard_map/all_gather | solution.py:123
  140.4 0.7 pad_maximum_fusion
  141.2 32.4 %all_gather.40 = bf16[1024,256]{1,0:T(8,128)(2,1)S(1)} all-gather(bf16[128,256]{1,0:T(8,128)(2,1)S(1)} %copy-done.1), channel_id=1, replica_groups=mesh['sp'=8,'tp'=4] {'sp'}, dimensions={0}, use_global_device_ids=true | all-gather | bytes 589824 | tf_op jit(solution)/shard_map/all_gather | solution.py:19
  174.1 5.4 %all_gather.41 = bf16[256,256]{1,0:T(8,128)(2,1)S(1)} all-gather(bf16[64,256]{1,0:T(8,128)(2,1)S(1)} %fusion.22), channel_id=1, replica_groups=mesh['sp'=8,'tp'=4] {'tp'}, dimensions={0}, use_global_device_ids=true | all-gather | bytes 163840 | tf_op jit(solution)/shard_map/all_gather | solution.py:24
  179.5 31.0 %all_gather.42 = bf16[256,384]{1,0:T(8,128)(2,1)S(1)} all-gather(bf16[32,384]{1,0:T(8,128)(2,1)S(1)} %copy-done.3), channel_id=1, replica_groups=mesh['sp'=8,'tp'=4] {'sp'}, dimensions={0}, use_global_device_ids=true | all-gather | bytes 221184 | tf_op jit(solution)/shard_map/all_gather | solution.py:122
  210.9 19.9 %all-gather = bf16[8,1,256]{2,1,0:T(2,128)(2,1)S(1)} all-gather(bf16[1,1,256]{2,1,0:T(2,128)(2,1)S(1)} %reshape.152), channel_id=1, replica_groups=mesh['sp'=8,'tp'=4] {'sp'}, dimensions={0}, use_global_device_ids=true | all-gather | bytes 4608 | tf_op jit(solution)/shard_map/all_gather | solution.py:19
  231.1 31.7 %all_gather.43 = bf16[256,1024]{1,0:T(8,128)(2,1)S(1)} all-gather(bf16[256,128]{1,0:T(8,128)(2,1)S(1)} %copy-done.2), channel_id=1, replica_groups=mesh['sp'=8,'tp'=4] {'sp'}, dimensions={1}, use_global_device_ids=true | all-gather | bytes 589824 | tf_op jit(solution)/shard_map/all_gather | solution.py:204
  262.7 3.1 copy.46
  265.9 19.8 %while.15 = (s32[]{:T(128)}, f32[4,256]{1,0:T(4,128)S(1)}, f32[4,256]{1,0:T(4,128)S(1)}, f32[256,4,64]{0,2,1:T(8,128)S(1)}, f32[256]{0:T(256)S(1)}, /*index=5*/b...) while((s32[]{:T(128)}, f32[4,256]{1,0:T(4,128)S(1)}, ...), condition=%wide.region_5.6_spmd.clone, body=%wide.region_2.5_spmd.clone.sunk | while | flops 86776064 | bytes 7655041 | solution.py:74
  265.9 1.0 dynamic-slice_bitcast_fusion.2
  268.3 1.0 dynamic-slice_bitcast_fusion.2
  270.8 1.0 dynamic-slice_bitcast_fusion.2
  272.3 0.4 select_reduce_fusion.2
  273.3 1.0 dynamic-slice_bitcast_fusion.2
  274.8 0.4 select_reduce_fusion.2
  275.8 1.0 dynamic-slice_bitcast_fusion.2
  277.3 0.4 select_reduce_fusion.2
  278.2 1.0 dynamic-slice_bitcast_fusion.2
  279.7 0.4 select_reduce_fusion.2
  280.7 1.0 dynamic-slice_bitcast_fusion.2
  283.2 1.0 dynamic-slice_bitcast_fusion.2
  284.7 0.4 select_reduce_fusion.2
  285.7 1.1 convolution_convert_fusion
  286.9 0.6 add_bitcast_fusion
  287.5 18.1 %reduce-scatter.2.cloned.1.call-done = bf16[64,1024]{1,0:T(8,128)(2,1)} async-done(((bf16[256,1024]{1,0:T(8,128)(2,1)}), bf16[64,1024]{1,0:T(8,128)(2,1)}) %reduce-scatter.2.cloned.1.call-update) | async-done | bytes 131088 | tf_op jit(solution)/shard_map/reduce_scatter | solution.py:30
  305.6 1.0 fusion.12
  306.6 1.7 fusion.14
  (131 shorter events, 12.1 us)
Async XLA Ops:
  7.2 32.7 %copy-start = (bf16[64,1024]{1,0:T(8,128)(2,1)S(1)}, bf16[64,1024]{1,0:T(8,128)(2,1)}, u32[]{:S(2)}) copy-start(bf16[64,1024]{1,0:T(8,128)(2,1)} %param.14) | copy-start | bytes 393220
  7.2 102.4 %copy-start.4 = (bf16[32,256]{1,0:T(8,128)(2,1)S(1)}, bf16[32,256]{1,0:T(8,128)(2,1)}, u32[]{:S(2)}) copy-start(bf16[32,256]{1,0:T(8,128)(2,1)} %param.22) | copy-start | bytes 49156
  7.2 134.0 %copy-start.1 = (bf16[128,256]{1,0:T(8,128)(2,1)S(1)}, bf16[128,256]{1,0:T(8,128)(2,1)}, u32[]{:S(2)}) copy-start(bf16[128,256]{1,0:T(8,128)(2,1)} %param.16) | copy-start | bytes 196612
  7.2 255.5 %all-gather.3.cloned.1.call-start = ((), (), s32[]{:S(2)}) async-start(), calls=%async_computation.1 | async-start | bytes 2506752 | tf_op jit(solution)/shard_map/all_gather | solution.py:19
  71.8 102.2 %copy-start.6 = (f32[256]{0:T(256)S(1)}, f32[256]{0:T(256)}, u32[]{:S(2)}) copy-start(f32[256]{0:T(256)} %param.19) | copy-start | bytes 3076
  72.0 107.5 %copy-start.3 = (bf16[32,384]{1,0:T(8,128)(2,1)S(1)}, bf16[32,384]{1,0:T(8,128)(2,1)}, u32[]{:S(2)}) copy-start(bf16[32,384]{1,0:T(8,128)(2,1)} %param.21) | copy-start | bytes 73732
  109.5 101.4 %copy-start.7 = (s32[256]{0:T(256)S(1)}, s32[256]{0:T(256)}, u32[]{:S(2)}) copy-start(s32[256]{0:T(256)} %param.15) | copy-start | bytes 3076
  140.4 90.7 %copy-start.2 = (bf16[256,128]{1,0:T(8,128)(2,1)S(1)}, bf16[256,128]{1,0:T(8,128)(2,1)}, u32[]{:S(2)}) copy-start(bf16[256,128]{1,0:T(8,128)(2,1)} %param.24) | copy-start | bytes 196612
  141.1 164.4 %reduce-scatter.2.cloned.1.call-start = ((), (), s32[]{:S(2)}) async-start(), calls=%async_computation.2 | async-start | bytes 655360 | tf_op jit(solution)/shard_map/reduce_scatter | solution.py:30
  285.7 21.0 %copy-start.5 = (f32[1024]{0:T(1024)S(1)}, f32[1024]{0:T(1024)}, u32[]{:S(2)}) copy-start(f32[1024]{0:T(1024)} %param.25) | copy-start | bytes 12292
Sparse Core Ops, SparseCore 0:
  141.3 54.6 all-gather.2
  287.0 18.5 reduce-scatter.1
where the time goes:
time: 316 us; the launch traced here: 315 us
  blocking collectives  251 us (79%)
  waiting for transfers between devices  18.2 us (6%)
  between operations  14.3 us (5%)
  local copies, waits for them, and re-layouts  11.6 us (4%)
  matrix products  10.7 us (3%)
  other arithmetic  8.39 us (3%)
    all_gather x4, blocking collectives, folded(): lax.all_gather(part, axis, axis=dim, tiled=True)  116 us
    all_gather x1, blocking collectives, on_device(): output_full = lax.all_gather(output_weight, 'sp', axis=1, tiled=True)  31.7 us
    all_gather x1, blocking collectives, on_device(): lax.all_gather(up_query, 'sp', axis=0, tiled=True)  31 us
    all_gather x1, blocking collectives, on_device(): lax.all_gather(up_value, 'sp', axis=0, tiled=True)  30.7 us
    all_gather x1, blocking collectives, on_device(): lax.all_gather(up_key, 'sp', axis=0, tiled=True)  30.5 us
    reduce_scatter x1, waiting for transfers between devices, summed_rows(): lax.psum_scatter(everything.astype(jnp.bfloat16), axis, scatter_dimension...  18.1 us
    all_gather x2, blocking collectives, gathered_then(): whole = lax.all_gather(value, axis, axis=dim, tiled=True)  11 us
    squeeze x8, local copies, waits for them, and re-layouts, over_blocks(): carry, unused = lax.scan(advance, carry, pieces_split)  7.82 us
  transfers between devices with their start and end apart: 2, of which 1 were waited for; matrix products, arithmetic and copies ran while one was open for 1% of the time, Pallas kernels for 0%

commit v1 on v0

v1 whole, which is shorter than its diff:
```python
import functools
import math

import jax
import jax.numpy as jnp
import numpy as np
from jax import lax
from jax.experimental import pallas as pl
from jax.experimental.pallas import tpu as pltpu
from jax.sharding import PartitionSpec as P

NOPE = 64
ROPE = 32
VDIM = 64
THETA = 10000.0
EPS = 1e-06
MASKED = -1e30
MESH = pl.DeviceIdType.MESH
F32 = jnp.float32
BF16 = jnp.bfloat16


def dot(a, b):
    return jnp.dot(a, b, preferred_element_type=F32)


def rows_joined(blocks, flat):
    n, r, c = blocks.shape
    for j in range(n):
        flat[j * r : (j + 1) * r, :] = blocks[j]
    return flat


def rms_parts(parts, gains):
    wide = [part.astype(F32) for part in parts]
    width = sum(part.shape[-1] for part in parts)
    total = sum(jnp.sum(part * part, axis=-1, keepdims=True) for part in wide)
    scale = lax.rsqrt(total / width + EPS)
    return [(part * scale * gain).astype(BF16) for part, gain in zip(wide, gains)]


def tables(tokens, heads):
    half = ROPE // 2
    inverse = np.float32(THETA) ** (-np.arange(half, dtype=np.float32) / np.float32(half))
    angles = np.arange(tokens, dtype=np.float32)[:, None] * inverse.astype(np.float32)[None, :]
    turn = np.zeros((tokens, 256), np.float32)
    turn[:, :ROPE] = np.tile(np.cos(angles), (1, 2))
    turn[:, 128 : 128 + ROPE] = np.tile(np.sin(angles), (1, 2))
    width = NOPE + ROPE
    pick = np.zeros((heads * width, heads * 384), np.float32)
    eye = np.arange(NOPE)
    rot = np.arange(ROPE)
    for head in range(heads):
        pick[head * width + eye, head * 384 + (head % 2) * NOPE + eye] = 1
        pick[head * width + NOPE + rot, head * 384 + 128 + rot] = 1
        low = np.arange(half)
        pick[head * width + NOPE + half + low, head * 384 + 256 + low] = -1
        pick[head * width + NOPE + low, head * 384 + 256 + half + low] = 1
    pick_key = np.zeros((ROPE, 256), np.float32)
    pick_key[rot, rot] = 1
    pick_key[half + low, 128 + low] = -1
    pick_key[low, 128 + half + low] = 1
    return turn, pick, pick_key


def kernel(
    n, ntp, heads,
    tokens, docs, down_q, down_k, down_r, gain_q, gain_k, up_q, up_k, up_v, out_w, gain_o,
    turn, pick, pick_key,
    out, log_out,
    tok, wd, wr, uq, up, wo, qraw, kraw, krot, tab, sel, qs, values, scores, att, part, got_core, got_y, send_y, wd_flat, wr_flat, uq_flat, up_flat,
    loc, s_uq, r_uq, s_tok, r_tok, s_wd, r_wd, s_wr, r_wr, s_up, r_up, s_wo, r_wo,
    s_q, r_q, s_k, r_k, s_ky, r_ky, s_kc, r_kc, s_kr, r_kr, s_krc, r_krc, s_f, r_f,
):
    half = n // 2
    me = lax.axis_index("sp")
    t = lax.axis_index("tp")
    ny = ntp // 2
    y = t // 2
    yh = lax.rem(y, 2)
    core = lax.rem(t, 2)
    own = tokens.shape[0]
    block = ntp * own
    side = block // 2
    cols = wd.shape[-1]
    partner = me + 1 - 2 * lax.rem(me, 2)
    other_core = t + 1 - 2 * core
    other_y = (y + 1 - 2 * yh) * 2 + core

    def dev(sp, tp):
        return (sp, tp)

    x_dev = dev(partner, t)
    y_dev = dev(me, other_y)
    c_dev = dev(me, other_core)

    col = pl.multiple_of(yh * cols, cols)
    c_tok = pltpu.make_async_copy(tokens, tok.at[t], loc.at[0])
    c_wr = pltpu.make_async_copy(down_r, wr.at[me], loc.at[2])
    nq, nk = up_q.shape[1], up_k.shape[1]
    c_up = [
        pltpu.make_async_copy(up_q, uq.at[me], loc.at[3]),
        pltpu.make_async_copy(up_k, up.at[me, :, pl.ds(0, nk)], loc.at[4]),
        pltpu.make_async_copy(up_v, up.at[me, :, pl.ds(nk, nk)], loc.at[5]),
    ]
    c_wo = pltpu.make_async_copy(out_w, wo.at[me], loc.at[6])
    c_tab = pltpu.make_async_copy(turn.at[me], tab, loc.at[7])
    c_sel = pltpu.make_async_copy(pick, sel, loc.at[8])
    c_tok.start()

    @pl.when(core == 0)
    def _():
        pltpu.make_async_copy(down_k.at[:, pl.ds(col, cols)], wd.at[me], loc.at[1]).start()

    @pl.when(core == 1)
    def _():
        pltpu.make_async_copy(down_q.at[:, pl.ds(col, cols)], wd.at[me], loc.at[1]).start()

    c_wd = pltpu.make_async_copy(down_q.at[:, pl.ds(0, cols)], wd.at[me], loc.at[1])
    for copy in [c_wr] + c_up + [c_wo, c_tab, c_sel]:
        copy.start()

    barrier = pltpu.get_barrier_semaphore()
    for k in range(1, n):
        pl.semaphore_signal(barrier, inc=1, device_id=dev(lax.rem(me + k, n), t), device_id_type=MESH)
    for k in range(1, ntp):
        pl.semaphore_signal(barrier, inc=1, device_id=dev(me, lax.rem(t + k, ntp)), device_id_type=MESH)

    def rc(src, dst, s, r, device):
        return pltpu.make_async_remote_copy(
            src_ref=src, dst_ref=dst, send_sem=s, recv_sem=r, device_id=device, device_id_type=MESH
        )

    class Gather:
        def __init__(self, at, s, r):
            self.at, self.s, self.r = at, s, r

        def z(self, k):
            return rc(self.at(me), self.at(me), self.s.at[k], self.r.at[k], dev(lax.rem(me + 2 * k, n), t))

        def x(self, k):
            ref = self.at(lax.rem(me - 2 * k + n, n))
            return rc(ref, ref, self.s.at[half + k], self.r.at[half + k], x_dev)

        def start_z(self):
            for k in range(1, half):
                self.z(k).start()

        def from_z(self, k):
            ref = self.at(lax.rem(me - 2 * k + n, n))
            rc(ref, ref, self.s.at[k], self.r.at[k], x_dev).wait_recv()

        def from_x(self, k):
            ref = self.at(lax.rem(partner - 2 * k + n, n))
            rc(ref, ref, self.s.at[half + k], self.r.at[half + k], x_dev).wait_recv()

        def hand_on(self):
            for k in range(1, half):
                self.from_z(k)
                self.x(k).start()

        def rest(self):
            for k in range(half):
                self.from_x(k)

        def drain(self):
            for k in range(1, half):
                self.z(k).wait_send()
            for k in range(half):
                self.x(k).wait_send()

    g_wd = Gather(lambda i: wd.at[i], s_wd, r_wd)
    g_wr = Gather(lambda i: wr.at[i], s_wr, r_wr)
    g_uq = Gather(lambda i: uq.at[i], s_uq, r_uq)
    g_up = Gather(lambda i: up.at[i], s_up, r_up)
    g_wo = Gather(lambda i: wo.at[i], s_wo, r_wo)
    g_k = Gather(lambda i: kraw.at[i, yh], s_k, r_k)
    g_kr = Gather(lambda i: krot.at[i], s_kr, r_kr)

    c_wd.wait()
    c_wr.wait()
    c_tok.wait()
    pl.semaphore_wait(barrier, n - 1 + ntp - 1)

    def y_at(k):
        return lax.rem(y + k, ny) * 2 + core

    def tok_y(k):
        return rc(tok.at[t], tok.at[t], s_tok.at[k], r_tok.at[k], dev(me, y_at(k)))

    def tok_from(k):
        ref = tok.at[y_at(ny - k)]
        return rc(ref, ref, s_tok.at[k], r_tok.at[k], c_dev)

    def tok_c(k):
        ref = tok.at[y_at(ny - k)]
        return rc(ref, ref, s_tok.at[ny + k], r_tok.at[ny + k], c_dev)

    for k in range(1, ny):
        tok_y(k).start()
    g_wd.start_z()
    g_wd.x(0).start()

    @pl.when(core == 1)
    def _():
        g_wr.start_z()
        g_wr.x(0).start()

    tok_c(0).start()
    for copy in c_up:
        copy.wait()
    g_up.start_z()
    g_uq.start_z()
    g_wd.hand_on()

    @pl.when(core == 1)
    def _():
        g_wr.hand_on()

    g_up.x(0).start()
    g_uq.x(0).start()
    for k in range(1, ny):
        tok_from(k).wait_recv()
        tok_c(k).start()

    down = lax.broadcasted_iota(jnp.int32, (block, block), 0)
    across = lax.broadcasted_iota(jnp.int32, (block, block), 1)
    doc_row = jnp.broadcast_to(docs[...].astype(F32), (block, block))
    doc_col = jnp.sum(jnp.where(down == across, doc_row, 0.0), axis=-1, keepdims=True)
    lane = lax.broadcasted_iota(jnp.int32, (block, 128), 1)
    in_docs = (lane >= ROPE) & (lane < ROPE + n)
    same = doc_col == (lane - ROPE).astype(F32)
    key_docs = jnp.where(in_docs & same, 1.0, 0.0)
    query_docs = jnp.where(in_docs & jnp.logical_not(same), MASKED, 0.0)

    for k in range(ny):
        tok_c(k).wait_recv()
    g_wd.rest()
    block_tokens = tok[...].reshape(block, tok.shape[-1])
    raw = dot(block_tokens, rows_joined(wd, wd_flat)[...]).astype(BF16)
    c_tab.wait()

    q_y = rc(qraw.at[yh], qraw.at[yh], s_q.at[0], r_q.at[0], y_dev)
    q_c = rc(qraw.at[yh], qraw.at[yh], s_q.at[1], r_q.at[1], c_dev)
    q_f = rc(qraw.at[1 - yh], qraw.at[1 - yh], s_q.at[2], r_q.at[2], c_dev)

    def k_y(i, slot):
        return rc(kraw.at[i, yh], kraw.at[i, yh], s_ky.at[slot], r_ky.at[slot], y_dev)

    def k_from_y(i, slot):
        return rc(kraw.at[i, 1 - yh], kraw.at[i, 1 - yh], s_ky.at[slot], r_ky.at[slot], y_dev)

    def k_c(i, which, slot):
        ref = kraw.at[i, which]
        return rc(ref, ref, s_kc.at[slot], r_kc.at[slot], c_dev)

    def kr_c(i, slot):
        return rc(krot.at[i], krot.at[i], s_krc.at[slot], r_krc.at[slot], c_dev)

    def block_of(slot):
        if slot < half:
            return lax.rem(me - 2 * slot + n, n)
        return lax.rem(partner - 2 * (slot - half) + n, n)

    @pl.when(core == 0)
    def _():
        kraw[me, yh] = raw
        g_k.start_z()
        g_k.x(0).start()
        k_y(me, 0).start()
        k_c(me, yh, 0).start()

    @pl.when(core == 1)
    def _():
        qraw[yh] = raw
        q_y.start()
        q_c.start()
        g_wr.rest()
        rotary = dot(block_tokens, rows_joined(wr, wr_flat)[...]).astype(BF16)
        both = dot(rotary, pick_key[...])
        turned = both[:, :128] * tab[:, :128] + both[:, 128:] * tab[:, 128:] + key_docs
        packed = turned[:side] + pltpu.roll(turned[side:], 64, 1)
        krot[me] = packed.astype(BF16)
        g_kr.start_z()
        g_kr.x(0).start()
        kr_c(me, 0).start()
        q_y.wait_recv()
        q_f.start()

    g_up.hand_on()
    g_uq.hand_on()
    c_wo.wait()

    g_wo.start_z()

    @pl.when(core == 0)
    def _():
        for k in range(1, half):
            g_k.from_z(k)
            g_k.x(k).start()
            k_y(block_of(k), k).start()
            k_c(block_of(k), yh, k).start()

    @pl.when(core == 1)
    def _():
        for k in range(1, half):
            g_kr.from_z(k)
            g_kr.x(k).start()
            kr_c(block_of(k), k).start()

    g_wo.x(0).start()
    g_up.rest()
    g_uq.rest()

    @pl.when(core == 0)
    def _():
        q_c.wait_recv()
        q_f.wait_recv()

    c_sel.wait()
    gq = gain_q[...]
    lat = rms_parts([qraw[0], qraw[1]], [gq[:, :cols], gq[:, cols:]])
    rows_joined(up, up_flat)
    rows_joined(uq, uq_flat)
    projected = (dot(lat[0], uq_flat[:cols, :]) + dot(lat[1], uq_flat[cols:, :])).astype(BF16)
    for head in range(heads):
        laid = dot(projected, sel[:, head * 384 : (head + 1) * 384])
        turned = laid[:, 128:256] * tab[:, :128] + laid[:, 256:] * tab[:, 128:] + query_docs
        plain = laid[:, :128].astype(BF16)
        rows = pl.ds((head % 2) * block, block)
        qs[head // 2, 0, rows, :128] = plain
        qs[head // 2, 1, rows, :128] = plain
        qs[head // 2, 0, rows, 128:] = turned.astype(BF16)
        qs[head // 2, 1, rows, 128:] = pltpu.roll(turned, 64, 1).astype(BF16)

    gk = gain_k[...]
    for slot in range(n):
        i = block_of(slot)

        @pl.when(core == 0)
        def _(slot=slot, i=i):
            if slot >= half:
                g_k.from_x(slot - half)
                k_y(i, slot).start()
                k_c(i, yh, slot).start()
            k_from_y(i, slot).wait_recv()
            k_c(i, 1 - yh, n + slot).start()
            kr_c(i, slot).wait_recv()

        @pl.when(core == 1)
        def _(slot=slot, i=i):
            if slot >= half:
                g_kr.from_x(slot - half)
                kr_c(i, slot).start()
            k_c(i, yh, slot).wait_recv()
            k_c(i, 1 - yh, n + slot).wait_recv()

        if slot > 0 and slot < half:
            g_wo.from_z(slot)
            g_wo.x(slot).start()

        lat = rms_parts([kraw[i, 0], kraw[i, 1]], [gk[:, :cols], gk[:, cols:]])
        kv = (dot(lat[0], up_flat[:cols, :]) + dot(lat[1], up_flat[cols:, :])).astype(BF16)
        values[i] = kv[:, nk:]
        rot = krot[i]
        for pair in range(heads // 2):
            for s in range(2):
                keys = jnp.concatenate(
                    [kv[s * side : (s + 1) * side, pair * 128 : (pair + 1) * 128], rot], axis=1
                )
                scores[pair, i, :, s * side : (s + 1) * side] = lax.dot_general(
                    qs[pair, s], keys, (((1,), (1,)), ((), ())), preferred_element_type=F32
                )

    scale = 1.0 / math.sqrt(NOPE + ROPE)
    factor = scale * math.log2(math.e)
    head_lane = lax.broadcasted_iota(jnp.int32, (block, nk), 1) // VDIM
    attended = jnp.zeros((block, nk), F32)
    sums = []
    for head in range(heads):
        rows = pl.ds((head % 2) * block, block)
        top = scores[head // 2, 0, rows, :]
        for i in range(1, n):
            top = jnp.maximum(top, scores[head // 2, i, rows, :])
        top = jnp.max(top, axis=-1, keepdims=True)
        shift = top * factor
        total = jnp.zeros((block, block), F32)
        mixed = jnp.zeros((block, nk), F32)
        for i in range(n):
            weights = jnp.exp2(scores[head // 2, i, rows, :] * factor - shift)
            total = total + weights
            mixed = mixed + dot(weights.astype(BF16), values[i])
        weight_sum = jnp.sum(total, axis=-1, keepdims=True)
        attended = jnp.where(head_lane == head, mixed / weight_sum, attended)
        sums.append(top * scale + jnp.log(weight_sum))
    log_out[...] = jnp.concatenate(sums, axis=1)
    att[...] = attended.astype(BF16)

    g_wo.rest()

    def partial(owner):
        rows = att[pl.ds(pl.multiple_of(owner * own, own), own), :]
        return jnp.concatenate([dot(rows, wo[j]) for j in range(n)], axis=1)

    def f_c(k):
        return rc(part.at[k], got_core.at[k], s_f.at[k], r_f.at[k], c_dev)

    def f_y(k):
        return rc(send_y.at[k], got_y.at[k], s_f.at[ny + k], r_f.at[ny + k], dev(me, y_at(k)))

    order = list(range(1, ny)) + [0]
    for k in order:
        part[k] = partial(lax.rem(y + k, ny) * 2 + 1 - core).astype(BF16)
        f_c(k).start()
    for k in order[:-1]:
        far = partial(y_at(k))
        f_c(k).wait_recv()
        send_y[k] = (far + got_core[k].astype(F32)).astype(BF16)
        f_y(k).start()
    near = partial(t)
    f_c(0).wait_recv()
    near = near + got_core[0].astype(F32)
    for k in order[:-1]:
        f_y(k).wait_recv()
        near = near + got_y[k].astype(F32)
    out[...] = rms_parts([near.astype(BF16)], [gain_o[...]])[0]

    for k in range(ny):
        tok_c(k).wait_send()
        f_c(k).wait_send()
        if k > 0:
            tok_y(k).wait_send()
            f_y(k).wait_send()
    for gather in (g_wd, g_up, g_uq, g_wo):
        gather.drain()

    @pl.when(core == 0)
    def _():
        g_k.drain()
        for slot in range(n):
            k_y(block_of(slot), slot).wait_send()
            k_c(block_of(slot), yh, slot).wait_send()
            k_c(block_of(slot), 1 - yh, n + slot).wait_send()

    @pl.when(core == 1)
    def _():
        g_wr.drain()
        g_kr.drain()
        for slot in range(n):
            kr_c(block_of(slot), slot).wait_send()
        for copy in (q_y, q_c, q_f):
            copy.wait_send()


def on_device(n, ntp, tokens, doc_ids, down_q, down_k, down_r, gain_q, gain_k, up_q, up_k, up_v, out_w, gain_o):
    own, width = tokens.shape
    block = doc_ids.shape[0]
    heads = up_k.shape[1] // NOPE
    rank = down_k.shape[1]
    cols = rank // 2
    nq, nk, nv = up_q.shape[1], up_k.shape[1], up_v.shape[1]
    turn, pick, pick_key = tables(n * block, heads)
    turn = jnp.asarray(turn.reshape(n, block, 256))
    vmem = pl.BlockSpec(memory_space=pltpu.VMEM)
    hbm = pl.BlockSpec(memory_space=pl.ANY)
    dma = lambda k: pltpu.SemaphoreType.DMA((k,))
    scratch = [
        pltpu.VMEM((ntp, own, width), BF16),
        pltpu.VMEM((n, width // n, cols), BF16),
        pltpu.VMEM((n, width // n, down_r.shape[1]), BF16),
        pltpu.VMEM((n, up_q.shape[0], nq), BF16),
        pltpu.VMEM((n, up_q.shape[0], nk + nv), BF16),
        pltpu.VMEM((n,) + out_w.shape, BF16),
        pltpu.VMEM((2, block, cols), BF16),
        pltpu.VMEM((n, 2, block, cols), BF16),
        pltpu.VMEM((n, block // 2, 128), BF16),
        pltpu.VMEM((block, 256), F32),
        pltpu.VMEM(pick.shape, BF16),
        pltpu.VMEM((heads // 2, 2, 2 * block, 256), BF16),
        pltpu.VMEM((n, block, nv), BF16),
        pltpu.VMEM((heads // 2, n, 2 * block, block), F32),
        pltpu.VMEM((block, nv), BF16),
        pltpu.VMEM((ntp // 2, own, width), BF16),
        pltpu.VMEM((ntp // 2, own, width), BF16),
        pltpu.VMEM((ntp // 2, own, width), BF16),
        pltpu.VMEM((ntp // 2, own, width), BF16),
        pltpu.VMEM((width, cols), BF16),
        pltpu.VMEM((width, down_r.shape[1]), BF16),
        pltpu.VMEM((rank, nq), BF16),
        pltpu.VMEM((rank, nk + nv), BF16),
        dma(9), dma(n), dma(n), dma(ntp), dma(ntp),
        dma(n), dma(n), dma(n), dma(n), dma(n), dma(n), dma(n), dma(n),
        dma(3), dma(3), dma(n), dma(n), dma(n), dma(n),
        dma(2 * n), dma(2 * n), dma(n), dma(n), dma(n), dma(n), dma(ntp), dma(ntp),
    ]
    return pl.pallas_call(
        functools.partial(kernel, n, ntp, heads),
        out_shape=(
            jax.ShapeDtypeStruct((own, width), BF16),
            jax.ShapeDtypeStruct((block, heads), F32),
        ),
        in_specs=[hbm, vmem, hbm, hbm, hbm, vmem, vmem, hbm, hbm, hbm, hbm, vmem, hbm, hbm, vmem],
        out_specs=(vmem, vmem),
        scratch_shapes=scratch,
        compiler_params=pltpu.CompilerParams(
            collective_id=0, has_side_effects=True, vmem_limit_bytes=60 * 1024 * 1024
        ),
    )(
        tokens, doc_ids[None, :], down_q, down_k, down_r, gain_q[None, :], gain_k[None, :],
        up_q, up_k, up_v, out_w, gain_o[None, :],
        turn, jnp.asarray(pick, BF16), jnp.asarray(pick_key, BF16),
    )


def solution(mesh):
    assert mesh.shape["tp"] % 4 == 0 and mesh.shape["sp"] % 2 == 0 and mesh.shape["sp"] <= 32
    placed = (
        P(("sp", "tp"), None), P("sp"), P("sp", None), P("sp", None), P("sp", None), P(), P(),
        P("sp", "tp"), P("sp", "tp"), P("sp", "tp"), P("tp", "sp"), P(),
    )
    return jax.shard_map(
        functools.partial(on_device, mesh.shape["sp"], mesh.shape["tp"]),
        mesh=mesh,
        in_specs=placed,
        out_specs=(P(("sp", "tp"), None), P("sp", "tp")),
        check_vma=False,
    )
```

time: 316 us -> 61.9 us (0.20)
  blocking collectives: 251 us -> 0 us
  Pallas kernels: 0 us -> 56.4 us
  waiting for transfers between devices: 18.2 us -> 0 us
  between operations: 14.3 us -> 0.64 us
  matrix products: 10.7 us -> 0 us
  other arithmetic: 8.39 us -> 0 us
  local copies, waits for them, and re-layouts: 11.6 us -> 4.56 us
    all_gather x10 -> x0, blocking collectives: 251 us -> none  [the longest x4 116 us: folded(): lax.all_gather(part, axis, axis=dim, tiled=True)]
    pallas_call x0 -> x1, Pallas kernels: none -> 56.4 us  [on_device(): pl.pallas_call(functools.partial(kernel, n, ntp, heads), out_shape=(jax.S...]
    reduce_scatter x1 -> x0, waiting for transfers between devices: 18.1 us -> none  [summed_rows(): lax.psum_scatter(everything.astype(jnp.bfloat16), axis, scatter_dimension...]
    dot_general x31 -> x0, matrix products: 10.7 us -> none  [the longest x8 3.01 us: attend(): jnp.einsum('qhr,kr->hqk', query_turned, key_turned, preferred_element_typ...]
    squeeze x8 -> x0, local copies, waits for them, and re-layouts: 7.82 us -> none  [over_blocks(): carry, unused = lax.scan(advance, carry, pieces_split)]
  transfers between devices with their start and end apart: 2 -> 0, of which waited for: 1 -> 0; matrix products, arithmetic and copies ran while one was open for 1% -> 0% of each run, Pallas kernels for 0% -> 0%
where the time goes in v1:
time: 61.9 us; the launch traced here: 61.6 us
  Pallas kernels  56.4 us (91%)
  local copies, waits for them, and re-layouts  4.56 us (7%)
  between operations  0.64 us (1%)
    pallas_call x1, Pallas kernels, on_device(): pl.pallas_call(functools.partial(kernel, n, ntp, heads), out_shape=(jax.S...  56.4 us
    unnamed x2, local copies, waits for them, and re-layouts  2.98 us
    pallas_call x1, local copies, waits for them, and re-layouts, on_device(): pl.pallas_call(functools.partial(kernel, n, ntp, heads), out_shape=(jax.S...  1.58 us

profile of v1, /device:TPU:0, one launch (start us, length us, event | category | flops | bytes accessed | tf_op | source)
XLA Modules:
  0.0 61.6 jit_solution(868801150472641393)
XLA Ops:
  0.6 1.4 %copy.17.down_r = bf16[128,32]{1,0:T(8,128)(2,1)} copy(bf16[128,32]{0,1:T(8,128)(2,1)} %param.19) | data formatting | bytes 16384 | tf_op args[4]
  2.0 56.4 %shard_map.158 = (bf16[64,1024]{1,0:T(8,128)(2,1)}, f32[256,4]{1,0:T(8,128)}) custom-call(bf16[64,1024]{1,0:T(8,128)(2,1)} %tokens.1, s32[1,256]{1,0:T(1,128)} %bitcast.5, bf16[128,256]{1,0:T(8,128)(2,1)} %down_q.1, bf16[128,256]{1,0:T(8,128)(2,1)} %down_k.1, bf16[128,32]{1,0:T(8,128)(2,1)} %copy.17.down_r, f32[1,256]{1,0:T(1,128)} %bitcast.6, ...), custom_call_target="tpu_custom_call" | custom-call | tf_op jit(solution)/shard_map/pallas_call | solution.py:496
  58.4 1.6 %copy.18 = f32[256,4]{0,1:T(4,128)} copy(f32[256,4]{1,0:T(8,128)} %get-tuple-element.3) | data formatting | bytes 8192 | tf_op jit(solution)/shard_map/pallas_call | solution.py:496
  60.0 1.6 %copy.20 = bf16[64,1024]{1,0:T(8,128)(2,1)} copy(bf16[64,1024]{1,0:T(8,128)(2,1)} %get-tuple-element.6) | data formatting | bytes 262144
